TPU v7x, 32 devices: a whole 2x2x4 slice. The times are simulated.
32 devices in a mesh: sp: 16 (over z, y, x), tp: 2 (over core).
Axes of the slice: x: 2, y: 2, z: 4, core: 2. Of those that a mesh axis runs over, the one named last changes fastest.
Arguments:
- resid: bfloat16 [8192, 2048], P('sp'), may hold values from -6 to 6
- queries: bfloat16 [8192, 2048], P('sp', 'tp'), may hold values from -6 to 6
- keys: bfloat16 [8192, 512], P('sp', 'tp'), may hold values from -6 to 6
- values: bfloat16 [8192, 512], P('sp', 'tp'), may hold values from -6 to 6
- documents: int32 [8192], P('sp'), may hold values from 0 to 7, never falling along the last dimension, each value on 1 to 2048 neighbouring positions
- q_gain: float32 [64], replicated, may hold values from 0.5 to 6.5
- k_gain: float32 [64], replicated, may hold values from 0.5 to 6.5
- sink: float32 [32], P('tp'), may hold values from -1 to 5
- w_out: bfloat16 [2048, 2048], P('tp'), may hold values from -0.5 to 0.5
- n_gain: float32 [2048], replicated, may hold values from 0.1 to 1.9
- w_up: bfloat16 [2048, 8192], P('sp', 'tp'), may hold values from -0.125 to 0.125
- w_down: bfloat16 [8192, 2048], P('tp', 'sp'), may hold values from -0.0625 to 0.0625
Outputs:
- layer_out: bfloat16 [8192, 2048], P('sp')
All inputs are finite; a program needn't handle non-finite values.
Results may differ from a plain program's by a relative error of at most 0.018.
The roundings to bfloat16 on the way count: a program that leaves them out, or rounds other values in their place, can miss the bound.
Values may be sent and summed in bfloat16 or wider, within the bound.
A program may use at most 128 MiB of HBM per device.

v0:
```python
import jax
import jax.numpy as jnp
from jax import lax
from jax.sharding import PartitionSpec as P

WINDOW = 128


EPS = 1e-06


def extended(x, sides, width):
    for axis, dim in sides:
        count, length = (lax.axis_size(axis), x.shape[dim])
        up = [(i, (i + 1) % count) for i in range(count - 1)]
        down = [(j, i) for i, j in up]
        last = lax.slice_in_dim(x, length - width, length, axis=dim)
        initial = lax.slice_in_dim(x, 0, width, axis=dim)
        before = lax.ppermute(last, axis, up)
        after = lax.ppermute(initial, axis, down)
        x = jnp.concatenate([before, x, after], axis=dim)
    return x


def rms_scale(field, gain):
    wide = field.astype(jnp.float32)
    return wide * lax.rsqrt(jnp.mean(wide * wide, axis=-1, keepdims=True) + EPS) * gain


def mixer_partial(normed, w_up, w_down):
    upward = jnp.dot(
        normed, lax.all_gather(w_up, "sp", axis=0, tiled=True), preferred_element_type=jnp.float32
    )
    active = jnp.square(jax.nn.relu(upward)).astype(jnp.bfloat16)
    return jnp.dot(
        active, lax.all_gather(w_down, "sp", axis=1, tiled=True), preferred_element_type=jnp.float32
    )


def shards(
    resid, queries, keys, values, documents, q_gain, k_gain, sink, w_out, n_gain, w_up, w_down
):
    rows = resid.shape[0]
    head_size = q_gain.shape[0]
    heads_here = sink.shape[0]
    kv_here = keys.shape[1] // head_size
    group = heads_here // kv_here
    qnorm = rms_scale(queries.reshape(rows, kv_here, group, head_size), q_gain).astype(jnp.bfloat16)
    knorm = rms_scale(keys.reshape(rows, kv_here, head_size), k_gain).astype(jnp.bfloat16)
    vheads = values.reshape(rows, kv_here, head_size)
    doc_here = documents.astype(jnp.bfloat16)
    near_keys, near_values, near_docs = (
        extended(knorm, (("sp", 0),), WINDOW),
        extended(vheads, (("sp", 0),), WINDOW),
        extended(doc_here, (("sp", 0),), WINDOW),
    )
    offset = lax.axis_index("sp") * rows
    total = rows * lax.axis_size("sp")
    query_pos = offset + jnp.arange(rows, dtype=jnp.int32)
    key_pos = offset - WINDOW + jnp.arange(rows + 2 * WINDOW, dtype=jnp.int32)
    distance = key_pos[None, :] - query_pos[:, None]
    allowed = (jnp.abs(distance) <= WINDOW) & (key_pos[None, :] >= 0) & (key_pos[None, :] < total)
    allowed = allowed & (near_docs[None, :] == doc_here[:, None])
    heads_all = heads_here * lax.axis_size("tp")
    first_head = (lax.axis_index("tp") * heads_here).astype(jnp.float32)
    slopes = jnp.exp2(
        -8.0 * (first_head + jnp.arange(heads_here, dtype=jnp.float32) + 1.0) / heads_all
    )
    slopes = slopes.reshape(kv_here, group)
    sink_f = sink.reshape(kv_here, group)
    scores = jnp.einsum(
        "rkgd,skd->kgrs", qnorm, near_keys, preferred_element_type=jnp.float32
    ) * head_size ** (-0.5)
    scores = scores - slopes[:, :, None, None] * jnp.abs(distance).astype(jnp.float32)[None, None]
    scores = jnp.where(allowed[None, None], scores, jnp.float32(-1e30))
    highest = jnp.maximum(jnp.max(scores, axis=-1), sink_f[:, :, None])
    weights = jnp.exp(scores - highest[..., None])
    denom = jnp.sum(weights, axis=-1) + jnp.exp(sink_f[:, :, None] - highest)
    summed = jnp.einsum(
        "kgrs,skd->rkgd",
        weights.astype(jnp.bfloat16),
        near_values,
        preferred_element_type=jnp.float32,
    )
    attended = (
        (summed / denom.transpose(2, 0, 1)[..., None])
        .astype(jnp.bfloat16)
        .reshape(rows, heads_here * head_size)
    )
    head_mix = lax.psum(
        jnp.dot(attended, w_out, preferred_element_type=jnp.float32).astype(jnp.bfloat16), "tp"
    ).astype(jnp.float32)
    middle = (resid.astype(jnp.float32) + head_mix).astype(jnp.bfloat16)
    normed = rms_scale(middle, n_gain).astype(jnp.bfloat16)
    partial_sum = mixer_partial(normed, w_up, w_down)
    unit_mix = lax.psum(partial_sum.astype(jnp.bfloat16), "tp").astype(jnp.float32)
    return (middle.astype(jnp.float32) + unit_mix).astype(jnp.bfloat16)


def solution(mesh):
    placed = (
        P("sp", None),
        P("sp", "tp"),
        P("sp", "tp"),
        P("sp", "tp"),
        P("sp"),
        P(),
        P(),
        P("tp"),
        P("tp", None),
        P(),
        P("sp", "tp"),
        P("tp", "sp"),
    )
    return jax.shard_map(
        shards, mesh=mesh, in_specs=placed, out_specs=P("sp", None), check_vma=False
    )
```

profile of v0, /device:TPU:13, one launch (start us, length us, event | category | flops | bytes accessed | tf_op | source)
XLA Modules:
  0.0 588.5 jit_solution(10305533719375993461)
XLA Ops:
  7.4 0.7 convert_element_type.69
  8.1 0.5 fusion.45
  8.6 3.1 collective-permute-start.2
  11.8 3.1 collective-permute-start.3
  14.8 1.1 copy.22
  16.0 0.8 multiply_convert_fusion.1
  16.8 0.7 fusion.44
  17.5 2.2 collective-permute-start.4
  19.7 4.0 collective-permute-start.5
  23.6 0.9 fusion.43
  24.6 2.9 collective-permute-start
  27.5 0.6 fusion.37
  28.2 1.5 copy.23
  29.9 0.6 add_rsqrt_fusion
  30.6 0.3 fusion.20
  31.0 0.7 max.24
  31.9 3.3 collective-permute-start.1
  35.2 0.7 pad_maximum_fusion
  35.9 1.8 fusion.24
  37.7 12.5 %fusion.3 = (f32[4,4,512]{2,1,0:T(4,128)S(1)}, f32[4,768,512,4]{2,1,3,0:T(8,128)}) fusion(f32[512,768]{0,1:T(8,128)S(1)} %fusion.20, f32[4,4]{1,0:T(4,128)S(1)} %multiply_exponential_fusion, pred[512,768]{0,1:T(8,128)(4,1)S(1)} %fusion.24, bf16[512,4,4,64]{0,3,2,1:T(8,128)(2,1)S(1)} %bitcast.50, f32[64]{0:T(128)} %param.17, f32[512,4,4]{0,2,1:T(4,128)} %add_rsqrt_fusion, ...), kind=kOutput, calls=%fused_computation.5 | convolution fusion | flops 840032256 | bytes 28639552 | tf_op jit(solution)/shard_map/rkgd,skd->kgrs/dot_general | solution.py:71
  50.2 12.1 %fusion.1 = f32[4,4,512]{2,1,0:T(4,128)S(1)} fusion(f32[4,768,512,4]{2,1,3,0:T(8,128)} %get-tuple-element.12, f32[4,4,512]{2,1,0:T(4,128)S(1)} %broadcast_maximum_fusion, f32[512,768]{0,1:T(8,128)S(1)} %fusion.20, f32[4,4]{1,0:T(4,128)S(1)} %multiply_exponential_fusion, pred[512,768]{0,1:T(8,128)(4,1)S(1)} %fusion.24), kind=kLoop, calls=%fused_computation.3 | loop fusion | flops 37740544 | bytes 27197504 | tf_op jit(solution)/shard_map/reduce_sum | solution.py:78
  62.4 12.5 %fusion.15 = bf16[512,4,4,64]{0,3,2,1:T(8,128)(2,1)S(1)} fusion(f32[4,768,512,4]{2,1,3,0:T(8,128)} %get-tuple-element.12, f32[4,4,512]{2,1,0:T(4,128)S(1)} %broadcast_maximum_fusion, f32[512,768]{0,1:T(8,128)S(1)} %fusion.20, f32[4,4]{1,0:T(4,128)S(1)} %multiply_exponential_fusion, pred[512,768]{0,1:T(8,128)(4,1)S(1)} %fusion.24, ...), kind=kOutput, calls=%fused_computation.25 | convolution fusion | flops 845283328 | bytes 28639296 | tf_op jit(solution)/shard_map/kgrs,skd->rkgd/dot_general | solution.py:79
  74.9 3.8 convolution_convert_fusion
  78.8 0.5 all-gather.3.cloned.1.call-update
  79.4 0.5 all-gather.5.cloned.1.call-update
  80.1 24.4 %all-reduce.3.cloned.1.call-done = bf16[512,2048]{1,0:T(8,128)(2,1)} async-done(((bf16[512,2048]{1,0:T(8,128)(2,1)}), bf16[512,2048]{1,0:T(8,128)(2,1)}) %all-reduce.3.cloned.1.call-update) | async-done | bytes 2097168 | tf_op jit(solution)/shard_map/psum | solution.py:90
  104.5 2.3 fusion.7
  106.9 166.9 %all-gather.3.cloned.1.call-done = bf16[2048,4096]{1,0:T(8,128)(2,1)} async-done(((bf16[128,4096]{1,0:T(8,128)(2,1)}), bf16[2048,4096]{1,0:T(8,128)(2,1)}) %all-gather.3.cloned.1.call-update) | async-done | bytes 16777232 | tf_op jit(solution)/shard_map/all_gather | solution.py:32
  273.7 249.7 %all-gather.5.cloned.1.call-done = bf16[4096,2048]{1,0:T(8,128)(2,1)} async-done(((bf16[4096,128]{1,0:T(8,128)(2,1)}), bf16[4096,2048]{1,0:T(8,128)(2,1)}) %all-gather.5.cloned.1.call-update) | async-done | bytes 16777232 | tf_op jit(solution)/shard_map/all_gather | solution.py:36
  523.5 29.8 %convolution_convert_fusion.1 = bf16[512,2048]{1,0:T(8,128)(2,1)} fusion(bf16[4096,2048]{1,0:T(8,128)(2,1)} %all-gather.5.cloned.1.call-done, bf16[2048,4096]{1,0:T(8,128)(2,1)} %all-gather.3.cloned.1.call-done, f32[2048]{0:T(1024)S(1)} %copy-done.3, f32[512]{0:T(512)S(1)} %add_rsqrt_fusion.2, bf16[512,2048]{1,0:T(8,128)(2,1)} %all-reduce.3.cloned.1.call-done, ...), kind=kOutput, calls=%fused_computation.18 | convolution fusion | flops 17195597824 | bytes 39856128 | tf_op jit(solution)/shard_map/dot_general | solution.py:35
  553.3 23.0 %all-reduce.5.cloned.1.call-done = bf16[512,2048]{1,0:T(8,128)(2,1)} async-done(((bf16[512,2048]{1,0:T(8,128)(2,1)}), bf16[512,2048]{1,0:T(8,128)(2,1)}) %all-reduce.5.cloned.1.call-update) | async-done | bytes 2097168 | tf_op jit(solution)/shard_map/psum | solution.py:96
  576.3 4.8 fusion.10
  (32 shorter events, 1.3 us)
Async XLA Ops:
  7.4 23.5 %copy-start.1 = (bf16[512,256]{1,0:T(8,128)(2,1)S(1)}, bf16[512,256]{1,0:T(8,128)(2,1)}, u32[]{:S(2)}) copy-start(bf16[512,256]{1,0:T(8,128)(2,1)} %param.15) | copy-start | bytes 786436
  7.4 97.2 %all-reduce.3.cloned.1.call-start = ((), (), s32[]{:S(2)}) async-start(), calls=%async_computation | async-start | bytes 4194304 | tf_op jit(solution)/shard_map/psum | solution.py:90
  8.6 23.3 %collective-permute-start.2 = (bf16[128]{0:T(256)(128)(2,1)}, bf16[128]{0:T(256)(128)(2,1)}, u32[]{:S(2)}, u32[]{:S(2)}) collective-permute-start(bf16[128]{0:T(256)(128)(2,1)} %get-tuple-element.9), channel_id=1, source_target_pairs={{0,2},{2,4},{4,6},{6,8},{8,10},{10,12},{12,14},{14,16},{16,18},{18... | collective-permute-start | bytes 776 | tf_op jit(solution)/shard_map/ppermute | solution.py:19
  11.8 23.5 %collective-permute-start.3 = (bf16[128]{0:T(256)(128)(2,1)}, bf16[128]{0:T(256)(128)(2,1)}, u32[]{:S(2)}, u32[]{:S(2)}) collective-permute-start(bf16[128]{0:T(256)(128)(2,1)} %get-tuple-element.10), channel_id=1, source_target_pairs={{2,0},{4,2},{6,4},{8,6},{10,8},{12,10},{14,12},{16,14},{18,16},{20... | collective-permute-start | bytes 776 | tf_op jit(solution)/shard_map/ppermute | solution.py:20
  17.5 20.2 %collective-permute-start.4 = (bf16[128,4,64]{0,2,1:T(8,128)(2,1)}, bf16[128,4,64]{0,2,1:T(8,128)(2,1)}, u32[]{:S(2)}, u32[]{:S(2)}) collective-permute-start(bf16[128,4,64]{0,2,1:T(8,128)(2,1)} %get-tuple-element.7), channel_id=1, source_target_pairs={{0,2},{2,4},{4,6},{6,8},{8,10},{10,12},{12,14},{14,16},{16,18},{18... | collective-permute-start | bytes 196616 | tf_op jit(solution)/shard_map/ppermute | solution.py:19
  19.7 18.0 %collective-permute-start.5 = (bf16[128,4,64]{0,2,1:T(8,128)(2,1)}, bf16[128,4,64]{0,2,1:T(8,128)(2,1)}, u32[]{:S(2)}, u32[]{:S(2)}) collective-permute-start(bf16[128,4,64]{0,2,1:T(8,128)(2,1)} %get-tuple-element.8), channel_id=1, source_target_pairs={{2,0},{4,2},{6,4},{8,6},{10,8},{12,10},{14,12},{16,14},{18,16},{20... | collective-permute-start | bytes 196616 | tf_op jit(solution)/shard_map/ppermute | solution.py:20
  24.6 37.8 %collective-permute-start = (bf16[128,4,64]{0,2,1:T(8,128)(2,1)S(1)}, bf16[128,4,64]{0,2,1:T(8,128)(2,1)}, u32[]{:S(2)}, u32[]{:S(2)}) collective-permute-start(bf16[128,4,64]{0,2,1:T(8,128)(2,1)S(1)} %bitcast.52), channel_id=1, source_target_pairs={{0,2},{2,4},{4,6},{6,8},{8,10},{10,12},{12,14},{14,16},{16,18},{18... | collective-permute-start | bytes 196616 | tf_op jit(solution)/shard_map/ppermute | solution.py:19
  31.9 30.5 %collective-permute-start.1 = (bf16[128,4,64]{0,2,1:T(8,128)(2,1)S(1)}, bf16[128,4,64]{0,2,1:T(8,128)(2,1)S(1)}, u32[]{:S(2)}, u32[]{:S(2)}) collective-permute-start(bf16[128,4,64]{0,2,1:T(8,128)(2,1)S(1)} %bitcast.53), channel_id=1, source_target_pairs={{2,0},{4,2},{6,4},{8,6},{10,8},{12,10},{14,12},{16,14},{18,16},{20... | collective-permute-start | bytes 196616 | tf_op jit(solution)/shard_map/ppermute | solution.py:20
  62.4 12.5 %copy-start.2 = (bf16[1024,2048]{1,0:T(8,128)(2,1)S(1)}, bf16[1024,2048]{1,0:T(8,128)(2,1)}, u32[]{:S(2)}) copy-start(bf16[1024,2048]{1,0:T(8,128)(2,1)} %param.20) | copy-start | bytes 12582916
  78.7 25.8 %copy-start = (bf16[512,2048]{1,0:T(8,128)(2,1)S(1)}, bf16[512,2048]{1,0:T(8,128)(2,1)}, u32[]{:S(2)}) copy-start(bf16[512,2048]{1,0:T(8,128)(2,1)} %param.12) | copy-start | bytes 6291460
  78.7 444.8 %copy-start.3 = (f32[2048]{0:T(1024)S(1)}, f32[2048]{0:T(1024)}, u32[]{:S(2)}) copy-start(f32[2048]{0:T(1024)} %param.21) | copy-start | bytes 24580
  78.7 195.0 %all-gather.3.cloned.1.call-start = ((), (), s32[]{:S(2)}) async-start(), calls=%async_computation.1 | async-start | bytes 17825792 | tf_op jit(solution)/shard_map/all_gather | solution.py:32
  79.3 444.1 %all-gather.5.cloned.1.call-start = ((), (), s32[]{:S(2)}) async-start(), calls=%async_computation.2 | async-start | bytes 17825792 | tf_op jit(solution)/shard_map/all_gather | solution.py:36
  79.9 496.4 %all-reduce.5.cloned.1.call-start = ((), (), s32[]{:S(2)}) async-start(), calls=%async_computation.3 | async-start | bytes 4194304 | tf_op jit(solution)/shard_map/psum | solution.py:96
Sparse Core Ops, SparseCore 0:
  78.9 25.6 all-reduce.2
  553.4 22.8 all-reduce.4
Sparse Core Ops, SparseCore 1:
  82.0 191.7 all-gather.2
  276.3 247.1 all-gather.4
where the time goes:
time: 590 us; the launch traced here: 589 us
  waiting for transfers between devices  465 us (79%)
  matrix products  58.5 us (10%)
  other arithmetic  25.2 us (4%)
  starting transfers between devices  18.8 us (3%)
  between operations  15.1 us (3%)
    all_gather x1, waiting for transfers between devices, mixer_partial(): lax.all_gather(w_down, 'sp', axis=1, tiled=True)  250 us
    all_gather x1, waiting for transfers between devices, mixer_partial(): lax.all_gather(w_up, 'sp', axis=0, tiled=True)  167 us
    dot_general x1, matrix products, mixer_partial(): jnp.dot(active, lax.all_gather(w_down, 'sp', axis=1, tiled=True), preferr...  29.8 us
    psum x1, waiting for transfers between devices, shards(): lax.psum(jnp.dot(attended, w_out, preferred_element_type=jnp.float32).ast...  24.4 us
    psum x1, waiting for transfers between devices, shards(): lax.psum(partial_sum.astype(jnp.bfloat16), 'tp').astype(jnp.float32)  23 us
    dot_general x1, matrix products, shards(): jnp.einsum('kgrs,skd->rkgd', weights.astype(jnp.bfloat16), near_values, p...  12.5 us
    dot_general x1, matrix products, shards(): jnp.einsum('rkgd,skd->kgrs', qnorm, near_keys, preferred_element_type=jnp...  12.5 us
    reduce_sum x1, other arithmetic, shards(): denom = jnp.sum(weights, axis=-1) + jnp.exp(sink_f[:, :, None] - highest)  12.1 us
  transfers between devices with their start and end apart: 10, of which 4 were waited for; matrix products, arithmetic and copies ran while one was open for 6% of the time, Pallas kernels for 0%

commit v1 on v0

--- a/solution.py
+++ b/solution.py
@@ -1,12 +1,443 @@
+import functools
+
 import jax
 import jax.numpy as jnp
 from jax import lax
+from jax.experimental import pallas as pl
+from jax.experimental.pallas import tpu as pltpu
 from jax.sharding import PartitionSpec as P
 
 WINDOW = 128
-
-
 EPS = 1e-06
+MEMBERS = 4
+F32 = jnp.float32
+BF16 = jnp.bfloat16
+MESH = pl.DeviceIdType.MESH
+
+
+def rms(wide, gain):
+    return wide * lax.rsqrt(jnp.mean(wide * wide, axis=-1, keepdims=True) + EPS) * gain
+
+
+def kernel(
+    n_sp,
+    head,
+    heads,
+    kv_heads,
+    resid,
+    queries,
+    keys,
+    values,
+    doc_col,
+    doc_row,
+    q_gain,
+    k_gain,
+    slopes,
+    sink,
+    w_out,
+    n_gain,
+    w_up,
+    w_down,
+    out,
+    kx,
+    vx,
+    dx,
+    kn,
+    att,
+    wo,
+    res,
+    mine,
+    other,
+    other_in,
+    mid,
+    normed,
+    wu,
+    wd,
+    act,
+    part,
+    twin_out,
+    twin_in,
+    sum_out,
+    sum_in,
+    half_out,
+    half_in,
+    halo_send,
+    halo_recv,
+    w_send,
+    w_recv,
+    w_local,
+    loc_sem,
+    tok_send,
+    tok_recv,
+    pair_send,
+    pair_recv,
+    misc_send,
+    misc_recv,
+):
+    rows = queries.shape[0]
+    half = rows // 2
+    depth = w_up.shape[0]
+    units = wu.shape[1]
+    width = wd.shape[1]
+    group = heads // kv_heads
+    n_za = n_sp // 8
+
+    sp = lax.axis_index("sp")
+    t = lax.axis_index("tp")
+    u = 1 - t
+    x = sp % 2
+    y = (sp // 2) % 2
+    zb = (sp // 4) % 2
+    za = sp // 8
+    me = zb * 2 + x
+
+    def index(za_, zb_, y_, x_):
+        return za_ * 8 + zb_ * 4 + y_ * 2 + x_
+
+    def flip(v, by):
+        return 1 - v if by else v
+
+    def remote(src, dst, send, recv, where):
+        return pltpu.make_async_remote_copy(
+            src_ref=src, dst_ref=dst, send_sem=send, recv_sem=recv,
+            device_id=where, device_id_type=MESH,
+        )
+
+    load_wo = pltpu.make_async_copy(w_out, wo, loc_sem.at[0])
+    load_wo.start()
+    load_res = pltpu.make_async_copy(resid.at[pl.ds(t * half, half), :], res, loc_sem.at[1])
+    load_res.start()
+    own_k = pltpu.make_async_copy(keys, kx.at[pl.ds(WINDOW, rows), :], loc_sem.at[2])
+    own_v = pltpu.make_async_copy(values, vx.at[pl.ds(WINDOW, rows), :], loc_sem.at[3])
+    own_d = pltpu.make_async_copy(doc_row, dx.at[:, pl.ds(WINDOW, rows)], loc_sem.at[4])
+    own_k.start()
+    own_v.start()
+    own_d.start()
+
+    def halo(side, where):
+        src = rows - WINDOW if side == 0 else 0
+        dst = 0 if side == 0 else WINDOW + rows
+        return [
+            remote(keys.at[pl.ds(src, WINDOW), :], kx.at[pl.ds(dst, WINDOW), :],
+                   halo_send.at[side, 0], halo_recv.at[side, 0], where),
+            remote(values.at[pl.ds(src, WINDOW), :], vx.at[pl.ds(dst, WINDOW), :],
+                   halo_send.at[side, 1], halo_recv.at[side, 1], where),
+            remote(doc_row.at[:, pl.ds(src, WINDOW)], dx.at[:, pl.ds(dst, WINDOW)],
+                   halo_send.at[side, 2], halo_recv.at[side, 2], where),
+        ]
+
+    up_to = lax.rem(sp + 1, n_sp)
+    down_to = lax.rem(sp + n_sp - 1, n_sp)
+
+    @pl.when(sp < n_sp - 1)
+    def _():
+        for c in halo(0, (up_to, t)):
+            c.start()
+
+    @pl.when(sp > 0)
+    def _():
+        for c in halo(1, (down_to, t)):
+            c.start()
+
+    def place(w, s):
+        if w == 0:
+            return wu.at[pl.ds(pl.multiple_of(s * depth, depth), depth), :]
+        return wd.at[:, pl.ds(pl.multiple_of(s * depth, depth), depth)]
+
+    def source(w, m):
+        at = pl.ds(pl.multiple_of(m * units, units), units)
+        return w_up.at[:, at] if w == 0 else w_down.at[at, :]
+
+    flips = ((0, 1), (1, 0), (1, 1))
+
+    def first_copy(w, k):
+        fz, fx = flips[k]
+        zb_, x_ = flip(zb, fz), flip(x, fx)
+        return remote(source(w, zb_ * 2 + x_), place(w, sp), w_send.at[w, k], w_recv.at[w, sp],
+                      (index(za, zb_, y, x_), t))
+
+    locals_ = [pltpu.make_async_copy(source(w, me), place(w, sp), w_local.at[w]) for w in range(2)]
+    for w in range(2):
+        for k in range(3):
+            first_copy(w, k).start()
+        locals_[w].start()
+
+    def forward(w, s, number, where):
+        return remote(place(w, s), place(w, s), w_send.at[w, number], w_recv.at[w, s], where)
+
+    def arrived(w, s):
+        remote(place(w, s), place(w, s), w_send.at[w, 0], w_recv.at[w, s], (sp, u)).wait_recv()
+
+    sent = [[], []]
+
+    def start(w, s, where):
+        number = 3 + len(sent[w])
+        c = forward(w, s, number, where)
+        c.start()
+        sent[w].append(c)
+
+    def spread(w):
+        for k in range(4):
+            if k == 0:
+                locals_[w].wait()
+                s = sp
+            else:
+                fz, fx = flips[k - 1]
+                s = index(za, flip(zb, fz), y, flip(x, fx))
+                arrived(w, s)
+            for d in range(1, n_za):
+                start(w, s, (index(lax.rem(za + d, n_za), zb, y, x), t))
+            start(w, s, (index(za, zb, 1 - y, x), t))
+
+    def relay(w):
+        for k in range(4):
+            fz, fx = ((0, 0),) [0] if k == 0 else flips[k - 1]
+            for d in range(1, n_za):
+                s = index(lax.rem(za + n_za - d, n_za), flip(zb, fz), y, flip(x, fx))
+                arrived(w, s)
+                start(w, s, (index(za, zb, 1 - y, x), t))
+
+    def finish(w):
+        for a in range(n_za):
+            for k in range(4):
+                arrived(w, index(a, k // 2, 1 - y, k % 2))
+
+    own_k.wait()
+    own_v.wait()
+    own_d.wait()
+
+    @pl.when(sp > 0)
+    def _():
+        for c in halo(0, (down_to, t)):
+            c.wait_recv()
+
+    @pl.when(sp == 0)
+    def _():
+        kx[pl.ds(0, WINDOW), :] = jnp.zeros((WINDOW, kx.shape[1]), BF16)
+        vx[pl.ds(0, WINDOW), :] = jnp.zeros((WINDOW, vx.shape[1]), BF16)
+        dx[:, pl.ds(0, WINDOW)] = jnp.full((8, WINDOW), -1, jnp.int32)
+
+    @pl.when(sp < n_sp - 1)
+    def _():
+        for c in halo(1, (up_to, t)):
+            c.wait_recv()
+
+    @pl.when(sp == n_sp - 1)
+    def _():
+        end = WINDOW + rows
+        kx[pl.ds(end, WINDOW), :] = jnp.zeros((WINDOW, kx.shape[1]), BF16)
+        vx[pl.ds(end, WINDOW), :] = jnp.zeros((WINDOW, vx.shape[1]), BF16)
+        dx[:, pl.ds(end, WINDOW)] = jnp.full((8, WINDOW), -1, jnp.int32)
+
+    def norm_keys(b, carry):
+        at = pl.ds(pl.multiple_of(b * WINDOW, WINDOW), WINDOW)
+        block = kx[at, :].astype(F32)
+        kn[at, :] = jnp.concatenate(
+            [rms(block[:, k * head:(k + 1) * head], k_gain[...]) for k in range(kv_heads)], axis=1
+        ).astype(BF16)
+        return carry
+
+    lax.fori_loop(0, kx.shape[0] // WINDOW, norm_keys, 0)
+
+    span = 3 * WINDOW
+
+    def attend(b, carry):
+        at = pl.ds(pl.multiple_of(b * WINDOW, WINDOW), WINDOW)
+        near = pl.ds(pl.multiple_of(b * WINDOW, WINDOW), span)
+        far = jnp.abs(
+            lax.broadcasted_iota(jnp.int32, (WINDOW, span), 1)
+            - lax.broadcasted_iota(jnp.int32, (WINDOW, span), 0) - WINDOW
+        )
+        allowed = (far <= WINDOW) & (dx[0:1, near] == doc_col[at, :])
+        mask = jnp.where(allowed, F32(0.0), F32(-1e30))
+        far = far.astype(F32)
+        for k in range(kv_heads):
+            lanes = slice(k * head, (k + 1) * head)
+            kb = kn[near, lanes]
+            vb = vx[near, lanes]
+            done = []
+            for g in range(group):
+                h = k * group + g
+                qb = rms(queries[at, h * head:(h + 1) * head].astype(F32), q_gain[...]).astype(BF16)
+                score = lax.dot_general(
+                    qb, kb, (((1,), (1,)), ((), ())), preferred_element_type=F32
+                ) * (head ** -0.5)
+                score = (score - slopes[h] * far) + mask
+                top = jnp.maximum(jnp.max(score, axis=-1, keepdims=True), sink[h])
+                p = jnp.exp(score - top)
+                denom = jnp.sum(p, axis=-1, keepdims=True) + jnp.exp(sink[h] - top)
+                summed = jnp.dot(p.astype(BF16), vb, preferred_element_type=F32)
+                done.append((summed / denom).astype(BF16))
+                if len(done) == 2:
+                    att[at, (h - 1) * head:(h + 1) * head] = jnp.concatenate(done, axis=1)
+                    done = []
+        return carry
+
+    blocks = rows // WINDOW
+    lax.fori_loop(0, blocks // 2, attend, 0)
+    spread(0)
+    lax.fori_loop(blocks // 2, blocks, attend, 0)
+    spread(1)
+
+    load_wo.wait()
+    tile = 256
+
+    def project(which, dest):
+        lhs = att[pl.ds(pl.multiple_of(which * half, half), half), :]
+
+        def step(j, carry):
+            cols = pl.ds(pl.multiple_of(j * tile, tile), tile)
+            dest[:, cols] = jnp.dot(lhs, wo[:, cols], preferred_element_type=F32).astype(BF16)
+            return carry
+
+        lax.fori_loop(0, width // tile, step, 0)
+
+    project(u, other)
+    swap = remote(other, other_in, misc_send.at[0], misc_recv.at[0], (sp, u))
+    swap.start()
+    project(t, mine)
+    load_res.wait()
+    swap.wait_recv()
+
+    def middle(i, carry):
+        at = pl.ds(pl.multiple_of(i * 64, 64), 64)
+        both = mine[at, :].astype(F32) + other_in[at, :].astype(F32)
+        value = (res[at, :].astype(F32) + both).astype(BF16)
+        mid[at, :] = value
+        normed[me * 2 + t, at, :] = rms(value.astype(F32), n_gain[...]).astype(BF16)
+        return carry
+
+    lax.fori_loop(0, half // 64, middle, 0)
+
+    def token_copy(k):
+        fz, fx = flips[k]
+        where = (index(za, flip(zb, fz), y, flip(x, fx)), t)
+        return remote(normed.at[me * 2 + t], normed.at[me * 2 + t], tok_send.at[k], tok_recv.at[k],
+                      where)
+
+    def token_arrival(k):
+        fz, fx = flips[k]
+        slot = (flip(zb, fz) * 2 + flip(x, fx)) * 2 + t
+        return slot, remote(normed.at[slot], normed.at[slot], tok_send.at[k], tok_recv.at[k], (sp, u))
+
+    def pair_copy(k, slot):
+        return remote(normed.at[slot], normed.at[slot], pair_send.at[k], pair_recv.at[k], (sp, u))
+
+    for k in range(3):
+        token_copy(k).start()
+    pair_copy(3, me * 2 + t).start()
+
+    relay(0)
+    for k in range(3):
+        slot, c = token_arrival(k)
+        c.wait_recv()
+        pair_copy(k, slot).start()
+    relay(1)
+    for k in range(3):
+        fz, fx = flips[k]
+        pair_copy(k, (flip(zb, fz) * 2 + flip(x, fx)) * 2 + u).wait_recv()
+    pair_copy(3, me * 2 + u).wait_recv()
+    finish(0)
+    finish(1)
+
+    def mix(slot, put):
+        lhs = normed[slot]
+
+        def up(j, carry):
+            cols = pl.ds(pl.multiple_of(j * tile, tile), tile)
+            v = jnp.maximum(jnp.dot(lhs, wu[:, cols], preferred_element_type=F32), 0.0)
+            act[:, cols] = (v * v).astype(BF16)
+            return carry
+
+        lax.fori_loop(0, units // tile, up, 0)
+        hidden = act[...]
+
+        def down(j, carry):
+            cols = pl.ds(pl.multiple_of(j * tile, tile), tile)
+            put(cols, jnp.dot(hidden, wd[:, cols], preferred_element_type=F32))
+            return carry
+
+        lax.fori_loop(0, width // tile, down, 0)
+
+    def twin_copy(i):
+        return remote(twin_out.at[i], twin_in.at[i], misc_send.at[1 + i], misc_recv.at[1 + i], (sp, u))
+
+    def sum_copy(i, where):
+        return remote(sum_out.at[i], sum_in.at[i], misc_send.at[5 + i], misc_recv.at[5 + i], where)
+
+    order = flips[::-1] + ((0, 0),)
+    sums = []
+    for i, (fz, fx) in enumerate(order):
+        zb_, x_ = flip(zb, fz), flip(x, fx)
+        slot = (zb_ * 2 + x_) * 2
+
+        def put_twin(cols, v, i=i):
+            twin_out[i, :, cols] = v.astype(BF16)
+
+        mix(slot + u, put_twin)
+        twin_copy(i).start()
+
+        def put_mine(cols, v):
+            part[:, cols] = v
+
+        mix(slot + t, put_mine)
+        twin_copy(i).wait_recv()
+        if i < 3:
+
+            def add(r, carry, i=i):
+                at = pl.ds(pl.multiple_of(r * 64, 64), 64)
+                sum_out[i, at, :] = (part[at, :] + twin_in[i, at, :].astype(F32)).astype(BF16)
+                return carry
+
+            lax.fori_loop(0, half // 64, add, 0)
+            c = sum_copy(i, (index(za, zb_, y, x_), t))
+            c.start()
+            sums.append(c)
+
+    for i in range(3):
+        sums[i].wait_recv()
+
+    def last(r, carry):
+        at = pl.ds(pl.multiple_of(r * 64, 64), 64)
+        total = part[at, :] + twin_in[3, at, :].astype(F32)
+        for i in range(3):
+            total = total + sum_in[i, at, :].astype(F32)
+        half_out[at, :] = (mid[at, :].astype(F32) + total).astype(BF16)
+        return carry
+
+    lax.fori_loop(0, half // 64, last, 0)
+    final = remote(half_out, half_in, misc_send.at[8], misc_recv.at[8], (sp, u))
+    final.start()
+    out[pl.ds(pl.multiple_of(t * half, half), half), :] = half_out[...]
+    final.wait_recv()
+    out[pl.ds(pl.multiple_of(u * half, half), half), :] = half_in[...]
+
+    final.wait_send()
+    swap.wait_send()
+
+    @pl.when(sp < n_sp - 1)
+    def _():
+        for c in halo(0, (up_to, t)):
+            c.wait_send()
+
+    @pl.when(sp > 0)
+    def _():
+        for c in halo(1, (down_to, t)):
+            c.wait_send()
+
+    for w in range(2):
+        for k in range(3):
+            first_copy(w, k).wait_send()
+        for c in sent[w]:
+            c.wait_send()
+    for k in range(3):
+        token_copy(k).wait_send()
+    for k in range(4):
+        pair_copy(k, me * 2 + t).wait_send()
+    for i in range(4):
+        twin_copy(i).wait_send()
+    for c in sums:
+        c.wait_send()
 
 
 def extended(x, sides, width):
@@ -37,7 +468,7 @@
     )
 
 
-def shards(
+def plain_shards(
     resid, queries, keys, values, documents, q_gain, k_gain, sink, w_out, n_gain, w_up, w_down
 ):
     rows = resid.shape[0]
@@ -97,6 +528,89 @@
     return (middle.astype(jnp.float32) + unit_mix).astype(jnp.bfloat16)
 
 
+def fused_shards(
+    resid, queries, keys, values, documents, q_gain, k_gain, sink, w_out, n_gain, w_up, w_down
+):
+    rows, width = resid.shape
+    half = rows // 2
+    n_sp = lax.axis_size("sp")
+    head = q_gain.shape[0]
+    heads = sink.shape[0]
+    kv_heads = keys.shape[1] // head
+    units = w_up.shape[1] // MEMBERS
+    n_za = n_sp // 8
+    first = (lax.axis_index("tp") * heads).astype(F32)
+    slopes = jnp.exp2(
+        -8.0 * (first + jnp.arange(heads, dtype=F32) + 1.0) / (heads * lax.axis_size("tp"))
+    )
+    vmem = pl.BlockSpec(memory_space=pltpu.VMEM)
+    smem = pl.BlockSpec(memory_space=pltpu.SMEM)
+    hbm = pl.BlockSpec(memory_space=pl.ANY)
+    sends = 3 + 4 * n_za + 4 * (n_za - 1)
+    dma = pltpu.SemaphoreType.DMA
+    return pl.pallas_call(
+        functools.partial(kernel, n_sp, head, heads, kv_heads),
+        out_shape=jax.ShapeDtypeStruct((rows, width), BF16),
+        in_specs=[hbm, vmem, vmem, vmem, vmem, vmem, vmem, vmem, smem, smem, hbm, vmem, hbm, hbm],
+        out_specs=vmem,
+        scratch_shapes=[
+            pltpu.VMEM((rows + 2 * WINDOW, keys.shape[1]), BF16),
+            pltpu.VMEM((rows + 2 * WINDOW, keys.shape[1]), BF16),
+            pltpu.VMEM((8, rows + 2 * WINDOW), jnp.int32),
+            pltpu.VMEM((rows + 2 * WINDOW, keys.shape[1]), BF16),
+            pltpu.VMEM((rows, heads * head), BF16),
+            pltpu.VMEM(w_out.shape, BF16),
+            pltpu.VMEM((half, width), BF16),
+            pltpu.VMEM((half, width), BF16),
+            pltpu.VMEM((half, width), BF16),
+            pltpu.VMEM((half, width), BF16),
+            pltpu.VMEM((half, width), BF16),
+            pltpu.VMEM((2 * MEMBERS, half, width), BF16),
+            pltpu.VMEM((width, units), BF16),
+            pltpu.VMEM((units, width), BF16),
+            pltpu.VMEM((half, units), BF16),
+            pltpu.VMEM((half, width), F32),
+            pltpu.VMEM((4, half, width), BF16),
+            pltpu.VMEM((4, half, width), BF16),
+            pltpu.VMEM((3, half, width), BF16),
+            pltpu.VMEM((3, half, width), BF16),
+            pltpu.VMEM((half, width), BF16),
+            pltpu.VMEM((half, width), BF16),
+            dma((2, 3)),
+            dma((2, 3)),
+            dma((2, sends)),
+            dma((2, n_sp)),
+            dma((2,)),
+            dma((5,)),
+            dma((3,)),
+            dma((3,)),
+            dma((4,)),
+            dma((4,)),
+            dma((9,)),
+            dma((9,)),
+        ],
+        compiler_params=pltpu.CompilerParams(
+            has_side_effects=True, vmem_limit_bytes=62 * 1024 * 1024
+        ),
+        name="layer",
+    )(
+        resid,
+        queries,
+        keys,
+        values,
+        documents[:, None],
+        jnp.broadcast_to(documents[None, :], (8, rows)),
+        q_gain[None, :],
+        k_gain[None, :],
+        slopes,
+        sink,
+        w_out,
+        n_gain[None, :],
+        w_up,
+        w_down,
+    )
+
+
 def solution(mesh):
     placed = (
         P("sp", None),
@@ -112,6 +626,13 @@
         P("sp", "tp"),
         P("tp", "sp"),
     )
+    sizes = dict(mesh.shape)
+
+    def shards(*args):
+        columns = args[11].shape[1]
+        fits = sizes["tp"] == 2 and sizes["sp"] % 8 == 0 and columns % 128 == 0
+        return (fused_shards if fits else plain_shards)(*args)
+
     return jax.shard_map(
         shards, mesh=mesh, in_specs=placed, out_specs=P("sp", None), check_vma=False
     )

time: 590 us -> 229 us (0.39)
  waiting for transfers between devices: 465 us -> 0 us
  Pallas kernels: 0 us -> 222 us
  matrix products: 58.5 us -> 0 us
  other arithmetic: 25.2 us -> 0.56 us
  starting transfers between devices: 18.8 us -> 0 us
  between operations: 15.1 us -> 0.01 us
    all_gather x2 -> x0, waiting for transfers between devices: 417 us -> none  [the longest x1 250 us: mixer_partial(): lax.all_gather(w_down, 'sp', axis=1, tiled=True)]
    pallas_call x0 -> x1, Pallas kernels: none -> 222 us  [fused_shards(): pl.pallas_call(functools.partial(kernel, n_sp, head, heads, kv_heads), ou...]
    dot_general x4 -> x0, matrix products: 58.5 us -> none  [the longest x1 29.8 us: mixer_partial(): jnp.dot(active, lax.all_gather(w_down, 'sp', axis=1, tiled=True), preferr...]
    psum x2 -> x0, waiting for transfers between devices: 47.4 us -> none  [the longest x1 24.4 us: shards(): lax.psum(jnp.dot(attended, w_out, preferred_element_type=jnp.float32).ast...]
    ppermute x6 -> x0, starting transfers between devices: 18.5 us -> none  [the longest x3 10.3 us: extended(): after = lax.ppermute(initial, axis, down)]
    reduce_sum x4 -> x0, other arithmetic: 14.7 us -> none  [the longest x1 12.1 us: shards(): denom = jnp.sum(weights, axis=-1) + jnp.exp(sink_f[:, :, None] - highest)]
    convert_element_type x4 -> x0, other arithmetic: 6.58 us -> none  [the longest x1 4.77 us: shards(): return (middle.astype(jnp.float32) + unit_mix).astype(jnp.bfloat16)]
  transfers between devices with their start and end apart: 10 -> 0, of which waited for: 4 -> 0; matrix products, arithmetic and copies ran while one was open for 6% -> 0% of each run, Pallas kernels for 0% -> 0%
where the time goes in v1:
time: 229 us
  Pallas kernels  222 us (97%)
  local copies, waits for them, and re-layouts  5.97 us (3%)
    pallas_call x1, Pallas kernels, fused_shards(): pl.pallas_call(functools.partial(kernel, n_sp, head, heads, kv_heads), ou...  222 us

profile of v1, /device:TPU:13, one launch (start us, length us, event | category | flops | bytes accessed | tf_op | source)
XLA Modules:
  0.0 228.6 jit_solution(3040153914086330728)
XLA Ops:
  0.0 0.6 multiply_exponential_fusion.slopes
  0.6 1.3 broadcast_in_dim.19.doc_row
  1.8 1.5 copy.13.doc_col
  3.4 222.0 %layer.1 = bf16[512,2048]{1,0:T(8,128)(2,1)} custom-call(bf16[512,2048]{1,0:T(8,128)(2,1)} %resid.1, bf16[512,1024]{1,0:T(8,128)(2,1)} %queries.1, bf16[512,256]{1,0:T(8,128)(2,1)} %keys.1, bf16[512,256]{1,0:T(8,128)(2,1)} %values.1, s32[512,1]{1,0:T(8,128)} %copy.13.doc_col, s32[8,512]{1,0:T(8,128)} %broadcast_in_dim.19.doc_row, f32[1,64]{1,0:T(1,128)} %bitcast.6, ...), custom_call_target="tpu_custom_call" | custom-call | tf_op jit(solution)/shard_map/layer/pallas_call | solution.py:551
  225.4 3.2 %copy.15 = bf16[512,2048]{1,0:T(8,128)(2,1)} copy(bf16[512,2048]{1,0:T(8,128)(2,1)} %layer.1) | data formatting | bytes 4194304

commit v2 on v1

--- a/solution.py
+++ b/solution.py
@@ -71,6 +71,8 @@
     tok_recv,
     pair_send,
     pair_recv,
+    swap_send,
+    swap_recv,
     misc_send,
     misc_recv,
 ):
@@ -102,6 +104,17 @@
             src_ref=src, dst_ref=dst, send_sem=send, recv_sem=recv,
             device_id=where, device_id_type=MESH,
         )
+
+    up_to = lax.rem(sp + 1, n_sp)
+    down_to = lax.rem(sp + n_sp - 1, n_sp)
+    partners = [(sp, u), (up_to, t), (down_to, t), (index(za, zb, 1 - y, x), t)]
+    partners += [(index(za, flip(zb, fz), y, flip(x, fx)), t) for fz, fx in ((0, 1), (1, 0), (1, 1))]
+    partners += [(index(lax.rem(za + d, n_za), zb, y, x), t) for d in range(1, n_za)]
+    with jax.named_scope("barrier"):
+        greeting = pltpu.get_barrier_semaphore()
+        for where in partners:
+            pl.semaphore_signal(greeting, inc=1, device_id=where, device_id_type=MESH)
+        pl.semaphore_wait(greeting, len(partners))
 
     load_wo = pltpu.make_async_copy(w_out, wo, loc_sem.at[0])
     load_wo.start()
@@ -126,9 +139,6 @@
                    halo_send.at[side, 2], halo_recv.at[side, 2], where),
         ]
 
-    up_to = lax.rem(sp + 1, n_sp)
-    down_to = lax.rem(sp + n_sp - 1, n_sp)
-
     @pl.when(sp < n_sp - 1)
     def _():
         for c in halo(0, (up_to, t)):
@@ -157,54 +167,59 @@
                       (index(za, zb_, y, x_), t))
 
     locals_ = [pltpu.make_async_copy(source(w, me), place(w, sp), w_local.at[w]) for w in range(2)]
-    for w in range(2):
+    def arrived(w, s):
+        remote(place(w, s), place(w, s), w_send.at[w, 0], w_recv.at[w, s], (sp, u)).wait_recv()
+
+    sent = [[], []]
+
+    def start(w, s, where, src=None):
+        c = remote(place(w, s) if src is None else src, place(w, s), w_send.at[w, 3 + len(sent[w])],
+                   w_recv.at[w, s], where)
+        c.start()
+        sent[w].append(c)
+
+    def onward(w, s, src=None):
+        for d in range(1, n_za):
+            start(w, s, (index(lax.rem(za + d, n_za), zb, y, x), t), src)
+        start(w, s, (index(za, zb, 1 - y, x), t), src)
+
+    def exchange(w):
         for k in range(3):
             first_copy(w, k).start()
         locals_[w].start()
 
-    def forward(w, s, number, where):
-        return remote(place(w, s), place(w, s), w_send.at[w, number], w_recv.at[w, s], where)
-
-    def arrived(w, s):
-        remote(place(w, s), place(w, s), w_send.at[w, 0], w_recv.at[w, s], (sp, u)).wait_recv()
-
-    sent = [[], []]
-
-    def start(w, s, where):
-        number = 3 + len(sent[w])
-        c = forward(w, s, number, where)
-        c.start()
-        sent[w].append(c)
+    def spread_own(w):
+        onward(w, sp, source(w, me))
 
     def spread(w):
-        for k in range(4):
-            if k == 0:
-                locals_[w].wait()
-                s = sp
-            else:
-                fz, fx = flips[k - 1]
+        with jax.named_scope(f"spread#w={w}"):
+            for fz, fx in flips:
                 s = index(za, flip(zb, fz), y, flip(x, fx))
                 arrived(w, s)
-            for d in range(1, n_za):
-                start(w, s, (index(lax.rem(za + d, n_za), zb, y, x), t))
-            start(w, s, (index(za, zb, 1 - y, x), t))
-
-    def relay(w):
-        for k in range(4):
-            fz, fx = ((0, 0),) [0] if k == 0 else flips[k - 1]
+                onward(w, s)
+
+    def relay(w, k):
+        fz, fx = ((0, 0),) [0] if k == 0 else flips[k - 1]
+        with jax.named_scope(f"relay#w={w}#k={k}"):
             for d in range(1, n_za):
                 s = index(lax.rem(za + n_za - d, n_za), flip(zb, fz), y, flip(x, fx))
                 arrived(w, s)
                 start(w, s, (index(za, zb, 1 - y, x), t))
 
     def finish(w):
-        for a in range(n_za):
-            for k in range(4):
-                arrived(w, index(a, k // 2, 1 - y, k % 2))
-
-    own_k.wait()
-    own_v.wait()
-    own_d.wait()
+        with jax.named_scope(f"finish#w={w}"):
+            locals_[w].wait()
+            for a in range(n_za):
+                for k in range(4):
+                    arrived(w, index(a, k // 2, 1 - y, k % 2))
+
+    exchange(0)
+    spread_own(0)
+
+    with jax.named_scope("own_wait"):
+        own_k.wait()
+        own_v.wait()
+        own_d.wait()
 
     @pl.when(sp > 0)
     def _():
@@ -237,7 +252,9 @@
         ).astype(BF16)
         return carry
 
-    lax.fori_loop(0, kx.shape[0] // WINDOW, norm_keys, 0)
+    exchange(1)
+    with jax.named_scope("norm_keys"):
+        lax.fori_loop(0, kx.shape[0] // WINDOW, norm_keys, 0)
 
     span = 3 * WINDOW
 
@@ -273,17 +290,12 @@
                     done = []
         return carry
 
-    blocks = rows // WINDOW
-    lax.fori_loop(0, blocks // 2, attend, 0)
-    spread(0)
-    lax.fori_loop(blocks // 2, blocks, attend, 0)
-    spread(1)
-
-    load_wo.wait()
     tile = 256
-
-    def project(which, dest):
-        lhs = att[pl.ds(pl.multiple_of(which * half, half), half), :]
+    rounds = half // WINDOW
+    swaps = []
+
+    def project(row, dest):
+        lhs = att[pl.ds(pl.multiple_of(row, WINDOW), WINDOW), :]
 
         def step(j, carry):
             cols = pl.ds(pl.multiple_of(j * tile, tile), tile)
@@ -292,72 +304,127 @@
 
         lax.fori_loop(0, width // tile, step, 0)
 
-    project(u, other)
-    swap = remote(other, other_in, misc_send.at[0], misc_recv.at[0], (sp, u))
-    swap.start()
-    project(t, mine)
-    load_res.wait()
-    swap.wait_recv()
-
-    def middle(i, carry):
-        at = pl.ds(pl.multiple_of(i * 64, 64), 64)
-        both = mine[at, :].astype(F32) + other_in[at, :].astype(F32)
-        value = (res[at, :].astype(F32) + both).astype(BF16)
-        mid[at, :] = value
-        normed[me * 2 + t, at, :] = rms(value.astype(F32), n_gain[...]).astype(BF16)
-        return carry
-
-    lax.fori_loop(0, half // 64, middle, 0)
-
-    def token_copy(k):
+    def token_rows(slot, r):
+        return normed.at[pl.ds(pl.multiple_of(slot * half + r * WINDOW, WINDOW), WINDOW), :]
+
+    def token_copy(k, r):
         fz, fx = flips[k]
         where = (index(za, flip(zb, fz), y, flip(x, fx)), t)
-        return remote(normed.at[me * 2 + t], normed.at[me * 2 + t], tok_send.at[k], tok_recv.at[k],
-                      where)
-
-    def token_arrival(k):
+        rows_ = token_rows(me * 2 + t, r)
+        return remote(rows_, rows_, tok_send.at[k, r], tok_recv.at[k, r], where)
+
+    def member(k):
+        if k == 3:
+            return me
         fz, fx = flips[k]
-        slot = (flip(zb, fz) * 2 + flip(x, fx)) * 2 + t
-        return slot, remote(normed.at[slot], normed.at[slot], tok_send.at[k], tok_recv.at[k], (sp, u))
-
-    def pair_copy(k, slot):
-        return remote(normed.at[slot], normed.at[slot], pair_send.at[k], pair_recv.at[k], (sp, u))
-
-    for k in range(3):
-        token_copy(k).start()
-    pair_copy(3, me * 2 + t).start()
-
-    relay(0)
-    for k in range(3):
-        slot, c = token_arrival(k)
-        c.wait_recv()
-        pair_copy(k, slot).start()
-    relay(1)
-    for k in range(3):
-        fz, fx = flips[k]
-        pair_copy(k, (flip(zb, fz) * 2 + flip(x, fx)) * 2 + u).wait_recv()
-    pair_copy(3, me * 2 + u).wait_recv()
+        return flip(zb, fz) * 2 + flip(x, fx)
+
+    def pair_copy(k, core, r):
+        rows_ = token_rows(member(k) * 2 + core, r)
+        return remote(rows_, rows_, pair_send.at[k, r], pair_recv.at[k, r], (sp, u))
+
+    def token_pass(k, r):
+        with jax.named_scope(f"token#k={k}#r={r}"):
+            rows_ = token_rows(member(k) * 2 + t, r)
+            remote(rows_, rows_, tok_send.at[k, r], tok_recv.at[k, r], (sp, u)).wait_recv()
+            if k == 1:
+                token_relay(r).start()
+            pair_copy(k, t, r).start()
+
+    def token_relay(r):
+        rows_ = token_rows(member(1) * 2 + t, r)
+        return remote(rows_, rows_, tok_send.at[2, r], tok_recv.at[2, r],
+                      (index(za, zb, y, 1 - x), t))
+
+    def one_round(r):
+        with jax.named_scope("project"):
+            project(u * half + r * WINDOW, other.at[r])
+            swap = remote(other.at[r], other_in.at[r], swap_send.at[r], swap_recv.at[r], (sp, u))
+            swap.start()
+            swaps.append(swap)
+            project(t * half + r * WINDOW, mine.at[r])
+        with jax.named_scope("swap_wait"):
+            swap.wait_recv()
+
+        def middle(i, carry):
+            at = pl.ds(pl.multiple_of(i * 64, 64), 64)
+            here = pl.ds(pl.multiple_of(r * WINDOW + i * 64, 64), 64)
+            both = mine[r, at, :].astype(F32) + other_in[r, at, :].astype(F32)
+            value = (res[here, :].astype(F32) + both).astype(BF16)
+            mid[here, :] = value
+            row = pl.multiple_of((me * 2 + t) * half + r * WINDOW + i * 64, 64)
+            normed[pl.ds(row, 64), :] = rms(value.astype(F32), n_gain[...]).astype(BF16)
+            return carry
+
+        lax.fori_loop(0, WINDOW // 64, middle, 0)
+        for k in (1, 0):
+            token_copy(k, r).start()
+        pair_copy(3, t, r).start()
+
+    def attend_pair(r, between):
+        with jax.named_scope("attend"):
+            lax.fori_loop(r, r + 1, attend, 0)
+        between()
+        with jax.named_scope("attend"):
+            lax.fori_loop(r + rounds, r + rounds + 1, attend, 0)
+
+    for r in range(rounds):
+        if r == 0:
+            attend_pair(r, lambda: spread(0))
+            spread_own(1)
+            load_wo.wait()
+            load_res.wait()
+        elif r == 1:
+            attend_pair(r, lambda: relay(0, 0))
+            relay(0, 1)
+        else:
+            attend_pair(r, lambda: None)
+        one_round(r)
+
+    def up(m):
+        row = pl.multiple_of(m * rows, rows)
+
+        def step(j, carry):
+            cols = pl.ds(pl.multiple_of(j * tile, tile), tile)
+            v = jnp.dot(normed[pl.ds(row, rows), :], wu[:, cols], preferred_element_type=F32)
+            v = jnp.maximum(v, 0.0)
+            act[pl.ds(row, rows), cols] = (v * v).astype(BF16)
+            return carry
+
+        with jax.named_scope("up"):
+            lax.fori_loop(0, units // tile, step, 0)
+
+    def pair_wait(k):
+        with jax.named_scope("pair_wait"):
+            for r in range(rounds):
+                pair_copy(k, u, r).wait_recv()
+
+    spread(1)
+    if rounds < 2:
+        relay(0, 0)
+        relay(0, 1)
+    for r in range(rounds - 1):
+        token_pass(1, r)
+    relay(0, 2)
+    relay(0, 3)
+    token_pass(1, rounds - 1)
+    relay(1, 0)
     finish(0)
+    pair_wait(3)
+    up(me)
+    for r in range(rounds):
+        token_pass(0, r)
+    relay(1, 1)
+    pair_wait(0)
+    up(member(0))
+    for r in range(rounds):
+        token_pass(2, r)
+    relay(1, 2)
+    relay(1, 3)
+    for k in (1, 2):
+        pair_wait(k)
+        up(member(k))
     finish(1)
-
-    def mix(slot, put):
-        lhs = normed[slot]
-
-        def up(j, carry):
-            cols = pl.ds(pl.multiple_of(j * tile, tile), tile)
-            v = jnp.maximum(jnp.dot(lhs, wu[:, cols], preferred_element_type=F32), 0.0)
-            act[:, cols] = (v * v).astype(BF16)
-            return carry
-
-        lax.fori_loop(0, units // tile, up, 0)
-        hidden = act[...]
-
-        def down(j, carry):
-            cols = pl.ds(pl.multiple_of(j * tile, tile), tile)
-            put(cols, jnp.dot(hidden, wd[:, cols], preferred_element_type=F32))
-            return carry
-
-        lax.fori_loop(0, width // tile, down, 0)
 
     def twin_copy(i):
         return remote(twin_out.at[i], twin_in.at[i], misc_send.at[1 + i], misc_recv.at[1 + i], (sp, u))
@@ -369,19 +436,21 @@
     sums = []
     for i, (fz, fx) in enumerate(order):
         zb_, x_ = flip(zb, fz), flip(x, fx)
-        slot = (zb_ * 2 + x_) * 2
-
-        def put_twin(cols, v, i=i):
-            twin_out[i, :, cols] = v.astype(BF16)
-
-        mix(slot + u, put_twin)
+        row = pl.multiple_of((zb_ * 2 + x_) * rows, rows)
+
+        def down(j, carry, i=i, row=row):
+            cols = pl.ds(pl.multiple_of(j * tile, tile), tile)
+            v = jnp.dot(act[pl.ds(row, rows), :], wd[:, cols], preferred_element_type=F32)
+            low, high = v[:half], v[half:]
+            twin_out[i, :, cols] = jnp.where(t == 0, high, low).astype(BF16)
+            part[:, cols] = jnp.where(t == 0, low, high)
+            return carry
+
+        with jax.named_scope("down"):
+            lax.fori_loop(0, width // tile, down, 0)
         twin_copy(i).start()
-
-        def put_mine(cols, v):
-            part[:, cols] = v
-
-        mix(slot + t, put_mine)
-        twin_copy(i).wait_recv()
+        with jax.named_scope("twin_wait"):
+            twin_copy(i).wait_recv()
         if i < 3:
 
             def add(r, carry, i=i):
@@ -394,8 +463,9 @@
             c.start()
             sums.append(c)
 
-    for i in range(3):
-        sums[i].wait_recv()
+    with jax.named_scope("sum_wait"):
+        for i in range(3):
+            sums[i].wait_recv()
 
     def last(r, carry):
         at = pl.ds(pl.multiple_of(r * 64, 64), 64)
@@ -406,14 +476,16 @@
         return carry
 
     lax.fori_loop(0, half // 64, last, 0)
-    final = remote(half_out, half_in, misc_send.at[8], misc_recv.at[8], (sp, u))
+    final = remote(half_out, half_in, misc_send.at[0], misc_recv.at[0], (sp, u))
     final.start()
     out[pl.ds(pl.multiple_of(t * half, half), half), :] = half_out[...]
-    final.wait_recv()
+    with jax.named_scope("final_wait"):
+        final.wait_recv()
     out[pl.ds(pl.multiple_of(u * half, half), half), :] = half_in[...]
 
     final.wait_send()
-    swap.wait_send()
+    for swap in swaps:
+        swap.wait_send()
 
     @pl.when(sp < n_sp - 1)
     def _():
@@ -430,10 +502,12 @@
             first_copy(w, k).wait_send()
         for c in sent[w]:
             c.wait_send()
-    for k in range(3):
-        token_copy(k).wait_send()
-    for k in range(4):
-        pair_copy(k, me * 2 + t).wait_send()
+    for r in range(rounds):
+        for k in range(2):
+            token_copy(k, r).wait_send()
+        token_relay(r).wait_send()
+        for k in range(4):
+            pair_copy(k, t, r).wait_send()
     for i in range(4):
         twin_copy(i).wait_send()
     for c in sums:
@@ -539,6 +613,7 @@
     kv_heads = keys.shape[1] // head
     units = w_up.shape[1] // MEMBERS
     n_za = n_sp // 8
+    rounds = half // WINDOW
     first = (lax.axis_index("tp") * heads).astype(F32)
     slopes = jnp.exp2(
         -8.0 * (first + jnp.arange(heads, dtype=F32) + 1.0) / (heads * lax.axis_size("tp"))
@@ -561,14 +636,14 @@
             pltpu.VMEM((rows, heads * head), BF16),
             pltpu.VMEM(w_out.shape, BF16),
             pltpu.VMEM((half, width), BF16),
+            pltpu.VMEM((rounds, WINDOW, width), BF16),
+            pltpu.VMEM((rounds, WINDOW, width), BF16),
+            pltpu.VMEM((rounds, WINDOW, width), BF16),
             pltpu.VMEM((half, width), BF16),
-            pltpu.VMEM((half, width), BF16),
-            pltpu.VMEM((half, width), BF16),
-            pltpu.VMEM((half, width), BF16),
-            pltpu.VMEM((2 * MEMBERS, half, width), BF16),
+            pltpu.VMEM((MEMBERS * rows, width), BF16),
             pltpu.VMEM((width, units), BF16),
             pltpu.VMEM((units, width), BF16),
-            pltpu.VMEM((half, units), BF16),
+            pltpu.VMEM((MEMBERS * rows, units), BF16),
             pltpu.VMEM((half, width), F32),
             pltpu.VMEM((4, half, width), BF16),
             pltpu.VMEM((4, half, width), BF16),
@@ -582,15 +657,17 @@
             dma((2, n_sp)),
             dma((2,)),
             dma((5,)),
-            dma((3,)),
-            dma((3,)),
-            dma((4,)),
-            dma((4,)),
-            dma((9,)),
-            dma((9,)),
+            dma((3, rounds)),
+            dma((3, rounds)),
+            dma((4, rounds)),
+            dma((4, rounds)),
+            dma((rounds,)),
+            dma((rounds,)),
+            dma((8,)),
+            dma((8,)),
         ],
         compiler_params=pltpu.CompilerParams(
-            has_side_effects=True, vmem_limit_bytes=62 * 1024 * 1024
+            collective_id=0, has_side_effects=True, vmem_limit_bytes=62 * 1024 * 1024
         ),
         name="layer",
     )(

time: 229 us -> 182 us (0.79)
  Pallas kernels: 222 us -> 174 us
    pallas_call x1, Pallas kernels: 222 us -> 174 us  [fused_shards(): pl.pallas_call(functools.partial(kernel, n_sp, head, heads, kv_heads), ou...]
where the time goes in v2:
time: 182 us; the launch traced here: 181 us
  Pallas kernels  174 us (96%)
  local copies, waits for them, and re-layouts  5.97 us (3%)
    pallas_call x1, Pallas kernels, fused_shards(): pl.pallas_call(functools.partial(kernel, n_sp, head, heads, kv_heads), ou...  174 us

profile of v2, /device:TPU:13, one launch (start us, length us, event | category | flops | bytes accessed | tf_op | source)
XLA Modules:
  0.0 180.9 jit_solution(3434733062447273961)
XLA Ops:
  0.0 0.6 multiply_exponential_fusion.slopes
  0.6 1.3 broadcast_in_dim.19.doc_row
  1.8 1.5 copy.13.doc_col
  3.4 174.4 %layer.1 = bf16[512,2048]{1,0:T(8,128)(2,1)} custom-call(bf16[512,2048]{1,0:T(8,128)(2,1)} %resid.1, bf16[512,1024]{1,0:T(8,128)(2,1)} %queries.1, bf16[512,256]{1,0:T(8,128)(2,1)} %keys.1, bf16[512,256]{1,0:T(8,128)(2,1)} %values.1, s32[512,1]{1,0:T(8,128)} %copy.13.doc_col, s32[8,512]{1,0:T(8,128)} %broadcast_in_dim.19.doc_row, f32[1,64]{1,0:T(1,128)} %bitcast.6, ...), custom_call_target="tpu_custom_call" | custom-call | tf_op jit(solution)/shard_map/layer/pallas_call | solution.py:626
  177.8 3.2 %copy.15 = bf16[512,2048]{1,0:T(8,128)(2,1)} copy(bf16[512,2048]{1,0:T(8,128)(2,1)} %layer.1) | data formatting | bytes 4194304
